TPU v7x, 32 devices: a whole 2x2x4 slice. The times are simulated.
32 devices in a mesh: grp: 2 (over x), ep: 16 (over z, y, core).
Axes of the slice: x: 2, y: 2, z: 4, core: 2. Of those that a mesh axis runs over, the one named last changes fastest.
Arguments:
- stream: bfloat16 [32, 2048], P('grp', 'ep'), parts along dimension 0, may hold values from -48 to 48
- conv_cache: bfloat16 [32, 3, 2560], P(('grp', 'ep')), parts along dimension 0, may hold values from -6 to 6
- scan_state: float32 [32, 32, 64, 128], P(('grp', 'ep')), parts along dimension 0, may hold values from -4 to 4
- gate_weight: bfloat16 [2048, 2048], P('ep'), may hold values from -0.125 to 0.125
- value_weight: bfloat16 [2048, 2048], P('ep'), may hold values from -0.125 to 0.125
- entry_weight: bfloat16 [2048, 256], P('ep'), may hold values from -0.125 to 0.125
- readout_weight: bfloat16 [2048, 256], P('ep'), may hold values from -0.125 to 0.125
- step_weight: bfloat16 [2048, 32], P('ep'), may hold values from -0.125 to 0.125
- conv_weight: bfloat16 [4, 2560], replicated, may hold values from -3 to 3
- step_bias: float32 [32], replicated, may hold values from -4 to -1
- decay_rate: float32 [32], replicated, may hold values from 0.5 to 8
- skip_gain: float32 [32], replicated, may hold values from 0.1 to 1.9
- group_gain: float32 [2048], replicated, may hold values from 0.1 to 1.9
- out_weight: bfloat16 [2048, 2048], P(None, 'ep'), may hold values from -0.125 to 0.125
- first_gain: float32 [2048], replicated, may hold values from 0.1 to 1.9
- routes: int32 [32, 4], P('grp'), parts along dimension 0, may hold values from 0 to 15, all different within a row; in each aligned block of 16 rows (0 to 15, 16 to 31, ...) at most 8 rows name the same one
- route_weight: float32 [32, 4], P('grp'), parts along dimension 0, may hold values from 0.1 to 1
- expert_gate: bfloat16 [16, 2048, 256], P('ep'), may hold values from -0.125 to 0.125
- expert_up: bfloat16 [16, 2048, 256], P('ep'), may hold values from -0.125 to 0.125
- expert_down: bfloat16 [16, 256, 2048], P('ep'), may hold values from -0.375 to 0.375
- shared_gate: bfloat16 [2048, 256], replicated, may hold values from -0.125 to 0.125
- shared_up: bfloat16 [2048, 256], replicated, may hold values from -0.125 to 0.125
- shared_down: bfloat16 [256, 2048], replicated, may hold values from -0.375 to 0.375
- second_gain: float32 [2048], P('ep'), may hold values from 0.1 to 1.9
Outputs:
- result: bfloat16 [32, 2048], P('grp', 'ep'), parts along dimension 0
- new_conv: bfloat16 [32, 3, 2560], P(('grp', 'ep')), parts along dimension 0
- new_state: float32 [32, 32, 64, 128], P(('grp', 'ep')), parts along dimension 0
There are 2 independent parts, one for each index of `grp`. A program takes and returns all parts, laid end to end along the dimension named above; an argument that names none is the same for every part. Nothing has to cross between parts.
Inputs may be any that keep to these rules, and one draw needn't show every extreme that they name: `routes`: each row names 4 different experts; no expert is named by more than 8 rows, a bound that some block reaches.
All inputs are finite; a program needn't handle non-finite values.
Results may differ from a plain program's by a relative error of at most 0.0065.
Values may be sent and summed in bfloat16 or wider, within the bound.
A program may use at most 64 MiB of HBM per device.

v0:
```python
import jax
import jax.numpy as jnp
from jax import lax
from jax.sharding import PartitionSpec as P

HEAD_DIM = 64
STATE = 128
GROUPS = 2
CAP = 8
RESIDUAL_SCALE = 2.0**0.25
NORM_EPSILON = 1e-05
GATED_EPSILON = 1e-06


def rounded(value):
    return lax.optimization_barrier(value.astype(jnp.bfloat16))


def finish_norm(residual, row_total, square, full_width, gain):
    mean_value = (row_total / full_width)[:, None]
    variance = (square / full_width)[:, None] - mean_value * mean_value
    return (residual - mean_value) * lax.rsqrt(variance + NORM_EPSILON) * gain


def swiglu(inputs, gate_matrix, up_matrix, down_matrix):
    hidden = (
        jax.nn.silu(jnp.dot(inputs, gate_matrix, preferred_element_type=jnp.float32))
        * jnp.dot(inputs, up_matrix, preferred_element_type=jnp.float32)
    ).astype(jnp.bfloat16)
    return rounded(jnp.dot(hidden, down_matrix, preferred_element_type=jnp.float32))


def on_device(
    stream,
    conv_cache,
    scan_state,
    gate_weight,
    value_weight,
    entry_weight,
    readout_weight,
    step_weight,
    conv_weight,
    step_bias,
    decay_rate,
    skip_gain,
    group_gain,
    out_weight,
    first_gain,
    routes,
    route_weight,
    expert_gate,
    expert_up,
    expert_down,
    shared_gate,
    shared_up,
    shared_down,
    second_gain,
):
    devices = lax.axis_size("ep")
    device_rank = lax.axis_index("ep")
    own_rows = conv_cache.shape[0]
    row_count = stream.shape[0]
    slice_width = stream.shape[1]
    full_width = slice_width * devices
    inner_width = gate_weight.shape[1]
    head_count = step_weight.shape[1]
    per_group = head_count // GROUPS
    group_width = inner_width // GROUPS
    bounds = (inner_width, 2 * inner_width + 2 * GROUPS * STATE)
    weights_in = (gate_weight, value_weight, entry_weight, readout_weight, step_weight)
    summed = rounded(
        lax.psum_scatter(
            jnp.concatenate(
                [
                    jnp.dot(stream, weight, preferred_element_type=jnp.float32)
                    for weight in weights_in
                ],
                axis=1,
            ),
            "ep",
            scatter_dimension=0,
            tiled=True,
        )
    )
    gate_rows = summed[:, : bounds[0]]
    fresh = summed[:, bounds[0] : bounds[1]]
    step_rows = summed[:, bounds[1] :]
    window = jnp.concatenate([conv_cache, fresh[:, None, :]], axis=1)
    active = jax.nn.silu(
        jnp.sum(window.astype(jnp.float32) * conv_weight.astype(jnp.float32)[None], axis=1)
    )
    head_in = active[:, :inner_width].reshape(own_rows, GROUPS, per_group, HEAD_DIM)
    entry_rows = active[:, inner_width : inner_width + GROUPS * STATE].reshape(
        own_rows, GROUPS, 1, 1, STATE
    )
    readout_rows = active[:, inner_width + GROUPS * STATE :].reshape(own_rows, GROUPS, 1, 1, STATE)
    step_size = jax.nn.softplus(step_rows.astype(jnp.float32) + step_bias).reshape(
        own_rows, GROUPS, per_group
    )
    retained = jnp.exp(-step_size * decay_rate.reshape(GROUPS, per_group))
    old_state = scan_state.reshape(own_rows, GROUPS, per_group, HEAD_DIM, STATE)
    new_state = (
        retained[..., None, None] * old_state
        + (step_size[..., None] * head_in)[..., None] * entry_rows
    )
    head_out = (
        jnp.sum(new_state * readout_rows, axis=-1)
        + skip_gain.reshape(GROUPS, per_group)[:, :, None] * head_in
    )
    gated_out = head_out.reshape(own_rows, GROUPS, group_width) * jax.nn.silu(
        gate_rows.astype(jnp.float32)
    ).reshape(own_rows, GROUPS, group_width)
    normed = gated_out * lax.rsqrt(
        jnp.mean(gated_out * gated_out, axis=-1, keepdims=True) + GATED_EPSILON
    )
    normed = (normed.reshape(own_rows, inner_width) * group_gain).astype(jnp.bfloat16)
    mixer_out = rounded(
        jnp.dot(
            lax.all_gather(normed, "ep", axis=0, tiled=True),
            out_weight,
            preferred_element_type=jnp.float32,
        )
    )
    column_start = device_rank * slice_width
    residual = RESIDUAL_SCALE * stream.astype(jnp.float32) + mixer_out.astype(jnp.float32)
    row_total, square = lax.psum(
        (jnp.sum(residual, axis=1), jnp.sum(residual * residual, axis=1)), "ep"
    )
    gain_part = lax.dynamic_slice_in_dim(first_gain, column_start, slice_width, 0)
    first_part = rounded(finish_norm(residual, row_total, square, full_width, gain_part))
    first_rows = lax.all_gather(first_part, "ep", axis=1, tiled=True)
    matches = routes[:, :, None] == jnp.arange(devices, dtype=jnp.int32)[None, None, :]
    member = jnp.sum(matches.astype(jnp.int32), axis=1)
    weight_of = jnp.sum(jnp.where(matches, route_weight[:, :, None], 0.0), axis=1)
    slot_rank = jnp.cumsum(member, axis=0) - member
    slot_ids = jnp.arange(CAP, dtype=jnp.int32)
    mine_member = lax.dynamic_slice_in_dim(member, device_rank, 1, 1)[:, 0]
    mine_slot = lax.dynamic_slice_in_dim(slot_rank, device_rank, 1, 1)[:, 0]
    chosen = (mine_slot[None, :] == slot_ids[:, None]) & (mine_member[None, :] == 1)
    taken_rows = jnp.dot(
        chosen.astype(jnp.bfloat16), first_rows, preferred_element_type=jnp.float32
    ).astype(jnp.bfloat16)
    expert_out = swiglu(taken_rows, expert_gate[0], expert_up[0], expert_down[0])
    arrived = lax.all_to_all(expert_out, "ep", split_axis=1, concat_axis=0, tiled=True)
    spread = jnp.where(
        (slot_rank[:, :, None] == slot_ids[None, None, :]) & (member[:, :, None] == 1),
        weight_of[:, :, None],
        0.0,
    )
    moe_part = jnp.dot(
        spread.reshape(row_count, devices * CAP),
        arrived.astype(jnp.float32),
        precision=lax.Precision.HIGHEST,
    )
    down_part = lax.dynamic_slice_in_dim(shared_down, column_start, slice_width, 1)
    shared_part = swiglu(first_rows, shared_gate, shared_up, down_part)
    moe_part = moe_part + shared_part.astype(jnp.float32)
    residual_two = RESIDUAL_SCALE * first_part.astype(jnp.float32) + moe_part
    total_two, square_two = lax.psum(
        (jnp.sum(residual_two, axis=1), jnp.sum(residual_two * residual_two, axis=1)), "ep"
    )
    result = finish_norm(residual_two, total_two, square_two, full_width, second_gain).astype(
        jnp.bfloat16
    )
    return (result, window[:, 1:], new_state.reshape(own_rows, head_count, HEAD_DIM, STATE))


def solution(mesh):
    return jax.shard_map(
        on_device,
        mesh=mesh,
        in_specs=(
            P("grp", "ep"),
            P(("grp", "ep"), None, None),
            P(("grp", "ep"), None, None, None),
            P("ep", None),
            P("ep", None),
            P("ep", None),
            P("ep", None),
            P("ep", None),
            P(),
            P(),
            P(),
            P(),
            P(),
            P(None, "ep"),
            P(),
            P("grp", None),
            P("grp", None),
            P("ep", None, None),
            P("ep", None, None),
            P("ep", None, None),
            P(),
            P(),
            P(),
            P("ep"),
        ),
        out_specs=(
            P("grp", "ep"),
            P(("grp", "ep"), None, None),
            P(("grp", "ep"), None, None, None),
        ),
        check_vma=False,
    )
```

profile of v0, /device:TPU:0, one launch (start us, length us, event | category | flops | bytes accessed | tf_op | source)
XLA Modules:
  0.0 191.0 jit_solution(8677031213126030681)
XLA Ops:
  0.7 0.7 copy-done.7
  1.4 1.3 convolution_dynamic-update-slice_fusion.1
  2.7 0.2 convolution_dynamic-update-slice_fusion
  2.9 1.0 convolution_dynamic-update-slice_fusion.3
  3.9 1.0 convolution_dynamic-update-slice_fusion.2
  4.9 0.8 convolution_dynamic-update-slice_fusion.4
  5.7 66.2 %all-reduce.4 = bf16[16,4640]{1,0:T(8,128)(2,1)S(1)} all-reduce(f32[16,4640]{1,0:T(8,128)S(1)} %convolution_dynamic-update-slice_fusion.4), channel_id=3, replica_groups=mesh['grp'=2,'ep'=16] {'ep'}, use_global_device_ids=true, to_apply=%region_0.0.clone | all-reduce | flops 74240 | bytes 445440
  71.9 0.6 copy-done.17
  72.6 0.6 dynamic-slice
  73.1 0.7 dynamic-slice_convert_fusion
  73.9 0.7 copy-done.8
  74.7 0.1 reshape.257
  74.8 0.6 copy-done.14
  75.4 0.1 broadcast_multiply_fusion
  75.5 1.4 multiply_reduce_fusion
  76.9 0.1 reduce_sum.91
  77.0 0.1 reduce_sum.90
  77.0 0.1 mul.271
  77.1 0.1 mul.272
  77.2 0.1 mul.277
  77.3 0.1 mul.273
  77.4 0.5 broadcast.167
  77.9 0.7 fusion.47
  78.6 0.1 multiply_reduce_fusion.4
  78.7 0.1 mul.281
  78.8 17.3 %all-gather = bf16[32768]{0:T(1024)(128)(2,1)S(1)} all-gather(bf16[2048]{0:T(1024)(128)(2,1)S(1)} %multiply_convert_fusion.2), channel_id=2, replica_groups=mesh['grp'=2,'ep'=16] {'ep'}, dimensions={0}, use_global_device_ids=true | all-gather | bytes 69632 | tf_op jit(solution)/shard_map/all_gather | solution.py:119
  96.2 1.3 convolution_convert_fusion.2
  97.5 0.1 fusion.33
  97.6 0.8 dynamic_slice.12
  98.4 31.4 %all-reduce.2 = (f32[16]{0:T(128)S(1)}, f32[16]{0:T(128)S(1)}) all-reduce(f32[16]{0:T(128)S(1)} %get-tuple-element.6, f32[16]{0:T(128)S(1)} %get-tuple-element.5), channel_id=1, replica_groups=mesh['grp'=2,'ep'=16] {'ep'}, use_global_device_ids=true, to_apply=%region_7.8 | all-reduce | flops 32 | bytes 256 | tf_op jit(solution)/shard_map/psum | solution.py:126
  129.8 0.1 multiply_convert_fusion.1
  129.9 17.3 %all_gather.7 = bf16[16,2048]{1,0:T(8,128)(2,1)S(1)} all-gather(bf16[16,128]{1,0:T(8,128)(2,1)S(1)} %multiply_convert_fusion.1), channel_id=1, replica_groups=mesh['grp'=2,'ep'=16] {'ep'}, dimensions={1}, use_global_device_ids=true | all-gather | bytes 69632 | tf_op jit(solution)/shard_map/all_gather | solution.py:131
  147.2 0.1 convert_reduce_fusion
  147.3 0.2 fusion.32
  147.5 0.2 dynamic-slice_reduce_fusion
  147.6 0.1 convolution_convert_fusion.1
  147.8 0.2 fusion.9
  148.1 1.3 convolution_convert_fusion
  149.4 3.6 %all-to-all-start = ((bf16[8,16,128]{2,0,1:T(8,128)(2,1)}), bf16[8,16,128]{2,0,1:T(8,128)(2,1)S(1)}, u32[]{:S(2)}, u32[]{:S(2)}) async-start(bf16[8,16,128]{2,0,1:T(8,128)(2,1)} %bitcast.13), calls=%async_computation | async-start | bytes 65536 | tf_op jit(solution)/shard_map/all_to_all | solution.py:144
  153.0 0.2 fusion.50
  153.3 1.2 fusion.5
  154.5 0.7 pad_maximum_fusion
  155.2 0.1 select_reduce_fusion
  155.3 4.3 %all-to-all-done = bf16[8,16,128]{2,0,1:T(8,128)(2,1)S(1)} async-done(((bf16[8,16,128]{2,0,1:T(8,128)(2,1)}), bf16[8,16,128]{2,0,1:T(8,128)(2,1)S(1)}, u32[]{:S(2)}, u32[]{:S(2)}) %all-to-all-start) | async-done | bytes 32800 | tf_op jit(solution)/shard_map/all_to_all | solution.py:144
  159.6 0.4 fusion.45
  160.0 29.7 %all-reduce.1 = (f32[16]{0:T(128)S(1)}, f32[16]{0:T(128)S(1)}) all-reduce(f32[16]{0:T(128)S(1)} %get-tuple-element.4, f32[16]{0:T(128)S(1)} %get-tuple-element.3), channel_id=1, replica_groups=mesh['grp'=2,'ep'=16] {'ep'}, use_global_device_ids=true, to_apply=%region_14.15 | all-reduce | flops 32 | bytes 256 | tf_op jit(solution)/shard_map/psum | solution.py:159
  189.7 0.7 copy-done.13
  190.3 0.7 multiply_convert_fusion
  (49 shorter events, 0.5 us)
Async XLA Ops:
  0.6 147.4 %copy-start = (bf16[1,256,2048]{2,1,0:T(8,128)(2,1)S(1)}, bf16[1,256,2048]{2,1,0:T(8,128)(2,1)}, u32[]{:S(2)}) copy-start(bf16[1,256,2048]{2,1,0:T(8,128)(2,1)} %param.43) | copy-start | bytes 3145732
  0.6 0.8 copy-start.7
  0.7 2.1 %copy-start.6 = (bf16[128,2048]{1,0:T(8,128)(2,1)S(1)}, bf16[128,2048]{1,0:T(8,128)(2,1)}, u32[]{:S(2)}) copy-start(bf16[128,2048]{1,0:T(8,128)(2,1)} %param.28) | copy-start | bytes 1572868
  1.4 74.1 %copy-start.1 = (f32[1,32,64,128]{3,2,1,0:T(8,128)S(1)}, f32[1,32,64,128]{3,2,1,0:T(8,128)}, u32[]{:S(2)}) copy-start(f32[1,32,64,128]{3,2,1,0:T(8,128)} %param.26) | copy-start | bytes 3145732
  71.9 0.7 copy-start.17
  73.1 0.7 copy-start.9
  73.8 0.7 copy-start.8
  74.7 0.7 copy-start.14
  74.7 0.7 copy-start.15
  75.5 1.6 copy-start.16
  75.5 3.3 %copy-start.11 = (f32[2048]{0:T(1024)S(1)}, f32[2048]{0:T(1024)}, u32[]{:S(2)}) copy-start(f32[2048]{0:T(1024)} %param.36) | copy-start | bytes 24580
  76.9 70.9 %copy-start.2 = (bf16[1,2048,256]{2,1,0:T(8,128)(2,1)S(1)}, bf16[1,2048,256]{2,1,0:T(8,128)(2,1)}, u32[]{:S(2)}) copy-start(bf16[1,2048,256]{2,1,0:T(8,128)(2,1)} %param.41) | copy-start | bytes 3145732
  78.8 68.3 %copy-start.10 = (s32[16,4]{0,1:T(4,128)S(1)}, s32[16,4]{0,1:T(4,128)}, u32[]{:S(2)}) copy-start(s32[16,4]{0,1:T(4,128)} %param.39) | copy-start | bytes 772
  96.1 51.9 %copy-start.3 = (bf16[1,2048,256]{2,1,0:T(8,128)(2,1)S(1)}, bf16[1,2048,256]{2,1,0:T(8,128)(2,1)}, u32[]{:S(2)}) copy-start(bf16[1,2048,256]{2,1,0:T(8,128)(2,1)} %param.42) | copy-start | bytes 3145732
  148.0 5.0 %copy-start.4 = (bf16[2048,256]{1,0:T(8,128)(2,1)S(1)}, bf16[2048,256]{1,0:T(8,128)(2,1)}, u32[]{:S(2)}) copy-start(bf16[2048,256]{1,0:T(8,128)(2,1)} %param.44) | copy-start | bytes 3145732
  149.4 3.9 %copy-start.5 = (bf16[2048,256]{1,0:T(8,128)(2,1)S(1)}, bf16[2048,256]{1,0:T(8,128)(2,1)}, u32[]{:S(2)}) copy-start(bf16[2048,256]{1,0:T(8,128)(2,1)} %param.45) | copy-start | bytes 3145732
  149.4 10.2 %all-to-all-start = ((bf16[8,16,128]{2,0,1:T(8,128)(2,1)}), bf16[8,16,128]{2,0,1:T(8,128)(2,1)S(1)}, u32[]{:S(2)}, u32[]{:S(2)}) async-start(bf16[8,16,128]{2,0,1:T(8,128)(2,1)} %bitcast.13), calls=%async_computation | async-start | bytes 65536 | tf_op jit(solution)/shard_map/all_to_all | solution.py:144
  154.5 0.7 copy-start.12
  189.7 0.7 copy-start.13
where the time goes:
time: 192 us; the launch traced here: 191 us
  blocking collectives  162 us (84%)
  matrix products  9.08 us (5%)
  local copies, waits for them, and re-layouts  6.89 us (4%)
  waiting for transfers between devices  4.33 us (2%)
  other arithmetic  4.32 us (2%)
  starting transfers between devices  3.63 us (2%)
    unnamed x1, blocking collectives  66.2 us
    psum x1, blocking collectives, on_device(): lax.psum((jnp.sum(residual, axis=1), jnp.sum(residual * residual, axis=1)...  31.4 us
    psum x1, blocking collectives, on_device(): lax.psum((jnp.sum(residual_two, axis=1), jnp.sum(residual_two * residual_...  29.7 us
    all_gather x1, blocking collectives, on_device(): lax.all_gather(normed, 'ep', axis=0, tiled=True)  17.3 us
    all_gather x1, blocking collectives, on_device(): first_rows = lax.all_gather(first_part, 'ep', axis=1, tiled=True)  17.3 us
    all_to_all x1, waiting for transfers between devices, on_device(): lax.all_to_all(expert_out, 'ep', split_axis=1, concat_axis=0, tiled=True)  4.33 us
    dot_general x5, matrix products, on_device(): jnp.dot(stream, weight, preferred_element_type=jnp.float32)  4.26 us
    unnamed x37, local copies, waits for them, and re-layouts  4.03 us
  transfers between devices with their start and end apart: 1, of which 1 were waited for; matrix products, arithmetic and copies ran while one was open for 1% of the time, Pallas kernels for 0%

commit v1 on v0

--- a/solution.py
+++ b/solution.py
@@ -10,6 +10,19 @@
 RESIDUAL_SCALE = 2.0**0.25
 NORM_EPSILON = 1e-05
 GATED_EPSILON = 1e-06
+
+
+def collect(shard, axis, dim):
+    ways = lax.axis_size(axis)
+    up = [(d, (d + 1) % ways) for d in range(ways)]
+    down = [(d, (d - 1) % ways) for d in range(ways)]
+    earlier, later = ([shard], [shard])
+    for _ in range(ways // 2):
+        earlier.append(lax.ppermute(earlier[-1], axis, up))
+    for _ in range((ways - 1) // 2):
+        later.append(lax.ppermute(later[-1], axis, down))
+    line = jnp.concatenate([*earlier[::-1], *later[1:]], axis=dim)
+    return jnp.roll(line, (lax.axis_index(axis) - ways // 2) * shard.shape[dim], axis=dim)
 
 
 def rounded(value):
@@ -115,11 +128,7 @@
     )
     normed = (normed.reshape(own_rows, inner_width) * group_gain).astype(jnp.bfloat16)
     mixer_out = rounded(
-        jnp.dot(
-            lax.all_gather(normed, "ep", axis=0, tiled=True),
-            out_weight,
-            preferred_element_type=jnp.float32,
-        )
+        jnp.dot(collect(normed, "ep", 0), out_weight, preferred_element_type=jnp.float32)
     )
     column_start = device_rank * slice_width
     residual = RESIDUAL_SCALE * stream.astype(jnp.float32) + mixer_out.astype(jnp.float32)

time: 192 us -> 218 us (1.14)
  starting transfers between devices: 3.63 us -> 34.6 us
  blocking collectives: 162 us -> 143 us
  waiting for transfers between devices: 4.33 us -> 18.3 us
    ppermute x0 -> x15, starting transfers between devices: none -> 31 us  [the longest x7 30.9 us: collect(): later.append(lax.ppermute(later[-1], axis, down))]
    all_gather x1 -> x0, blocking collectives: 17.3 us -> none  [on_device(): lax.all_gather(normed, 'ep', axis=0, tiled=True)]
    ppermute x0 -> x15, waiting for transfers between devices: none -> 13.2 us  [the longest x8 11.8 us: collect(): earlier.append(lax.ppermute(earlier[-1], axis, up))]
  transfers between devices with their start and end apart: 1 -> 16, of which waited for: 1 -> 11; matrix products, arithmetic and copies ran while one was open for 1% -> 2% of each run, Pallas kernels for 0% -> 0%
where the time goes in v1:
time: 218 us; the launch traced here: 217 us
  blocking collectives  143 us (66%)
  starting transfers between devices  34.6 us (16%)
  waiting for transfers between devices  18.3 us (8%)
  matrix products  9 us (4%)
  local copies, waits for them, and re-layouts  7.26 us (3%)
  other arithmetic  4.3 us (2%)
    unnamed x1, blocking collectives  66.2 us
    ppermute x7, starting transfers between devices, collect(): later.append(lax.ppermute(later[-1], axis, down))  30.9 us
    psum x1, blocking collectives, on_device(): lax.psum((jnp.sum(residual_two, axis=1), jnp.sum(residual_two * residual_...  29.7 us
    psum x1, blocking collectives, on_device(): lax.psum((jnp.sum(residual, axis=1), jnp.sum(residual * residual, axis=1)...  29.5 us
    all_gather x1, blocking collectives, on_device(): first_rows = lax.all_gather(first_part, 'ep', axis=1, tiled=True)  17.3 us
    ppermute x8, waiting for transfers between devices, collect(): earlier.append(lax.ppermute(earlier[-1], axis, up))  11.8 us
    all_to_all x1, waiting for transfers between devices, on_device(): lax.all_to_all(expert_out, 'ep', split_axis=1, concat_axis=0, tiled=True)  5.13 us
  transfers between devices with their start and end apart: 16, of which 11 were waited for; matrix products, arithmetic and copies ran while one was open for 2% of the time, Pallas kernels for 0%

profile of v1, /device:TPU:0, one launch (start us, length us, event | category | flops | bytes accessed | tf_op | source)
XLA Modules:
  0.0 217.1 jit_solution(16144294664697852760)
XLA Ops:
  0.7 0.7 copy-done.7
  1.4 1.3 convolution_dynamic-update-slice_fusion.1
  2.9 1.0 convolution_dynamic-update-slice_fusion.3
  3.9 1.0 convolution_dynamic-update-slice_fusion.2
  4.9 0.8 convolution_dynamic-update-slice_fusion.4
  5.7 66.2 %all-reduce.4 = bf16[16,4640]{1,0:T(8,128)(2,1)S(1)} all-reduce(f32[16,4640]{1,0:T(8,128)S(1)} %convolution_dynamic-update-slice_fusion.4), channel_id=2, replica_groups=mesh['grp'=2,'ep'=16] {'ep'}, use_global_device_ids=true, to_apply=%region_0.0.clone | all-reduce | flops 74240 | bytes 445440
  71.9 0.6 copy-done.17
  72.6 0.6 dynamic-slice
  73.1 0.7 dynamic-slice_convert_fusion
  73.9 0.7 copy-done.8
  74.8 0.6 copy-done.14
  75.5 1.4 multiply_reduce_fusion
  77.4 0.5 broadcast.168
  77.9 0.7 fusion.49
  78.9 4.4 %collective-permute-start.8 = (bf16[1,2048]{1,0:T(2,128)(2,1)S(1)}, bf16[1,2048]{1,0:T(2,128)(2,1)S(1)}, u32[]{:S(2)}, u32[]{:S(2)}) collective-permute-start(bf16[1,2048]{1,0:T(2,128)(2,1)S(1)} %convert_element_type.70), channel_id=1, source_target_pairs={{0,15},{1,0},{2,1},{3,2},{4,3},{5,4},{6,5},{7,6},{8,7},{9,8},{10,9... | collective-permute-start | bytes 12296 | tf_op jit(solution)/shard_map/ppermute | solution.py:23
  83.4 1.3 collective-permute-done
  84.7 4.4 %collective-permute-start.9 = (bf16[1,2048]{1,0:T(2,128)(2,1)S(1)}, bf16[1,2048]{1,0:T(2,128)(2,1)S(1)}, u32[]{:S(2)}, u32[]{:S(2)}) collective-permute-start(bf16[1,2048]{1,0:T(2,128)(2,1)S(1)} %collective-permute-done.8), channel_id=1, source_target_pairs={{0,15},{1,0},{2,1},{3,2},{4,3},{5,4},{6,5},{7,6},{8,7},{9,8},{10,9... | collective-permute-start | bytes 12296 | tf_op jit(solution)/shard_map/ppermute | solution.py:23
  89.1 1.3 collective-permute-done.1
  90.5 4.4 %collective-permute-start.10 = (bf16[1,2048]{1,0:T(2,128)(2,1)S(1)}, bf16[1,2048]{1,0:T(2,128)(2,1)S(1)}, u32[]{:S(2)}, u32[]{:S(2)}) collective-permute-start(bf16[1,2048]{1,0:T(2,128)(2,1)S(1)} %collective-permute-done.9), channel_id=1, source_target_pairs={{0,15},{1,0},{2,1},{3,2},{4,3},{5,4},{6,5},{7,6},{8,7},{9,8},{10,9... | collective-permute-start | bytes 12296 | tf_op jit(solution)/shard_map/ppermute | solution.py:23
  94.9 1.3 collective-permute-done.2
  96.3 4.4 %collective-permute-start.11 = (bf16[1,2048]{1,0:T(2,128)(2,1)S(1)}, bf16[1,2048]{1,0:T(2,128)(2,1)S(1)}, u32[]{:S(2)}, u32[]{:S(2)}) collective-permute-start(bf16[1,2048]{1,0:T(2,128)(2,1)S(1)} %collective-permute-done.10), channel_id=1, source_target_pairs={{0,15},{1,0},{2,1},{3,2},{4,3},{5,4},{6,5},{7,6},{8,7},{9,8},{10,9... | collective-permute-start | bytes 12296 | tf_op jit(solution)/shard_map/ppermute | solution.py:23
  100.7 1.3 collective-permute-done.3
  102.0 0.6 pad_maximum_fusion
  102.7 4.4 %collective-permute-start.12 = (bf16[1,2048]{1,0:T(2,128)(2,1)S(1)}, bf16[1,2048]{1,0:T(2,128)(2,1)S(1)}, u32[]{:S(2)}, u32[]{:S(2)}) collective-permute-start(bf16[1,2048]{1,0:T(2,128)(2,1)S(1)} %collective-permute-done.11), channel_id=1, source_target_pairs={{0,15},{1,0},{2,1},{3,2},{4,3},{5,4},{6,5},{7,6},{8,7},{9,8},{10,9... | collective-permute-start | bytes 12296 | tf_op jit(solution)/shard_map/ppermute | solution.py:23
  107.1 0.7 collective-permute-done.4
  107.9 0.6 collective-permute-done.12
  108.5 4.4 %collective-permute-start.13 = (bf16[1,2048]{1,0:T(2,128)(2,1)S(1)}, bf16[1,2048]{1,0:T(2,128)(2,1)S(1)}, u32[]{:S(2)}, u32[]{:S(2)}) collective-permute-start(bf16[1,2048]{1,0:T(2,128)(2,1)S(1)} %collective-permute-done.12), channel_id=1, source_target_pairs={{0,15},{1,0},{2,1},{3,2},{4,3},{5,4},{6,5},{7,6},{8,7},{9,8},{10,9... | collective-permute-start | bytes 12296 | tf_op jit(solution)/shard_map/ppermute | solution.py:23
  112.9 0.7 collective-permute-done.5
  113.6 0.7 collective-permute-done.13
  114.2 4.4 %collective-permute-start.14 = (bf16[1,2048]{1,0:T(2,128)(2,1)S(1)}, bf16[1,2048]{1,0:T(2,128)(2,1)S(1)}, u32[]{:S(2)}, u32[]{:S(2)}) collective-permute-start(bf16[1,2048]{1,0:T(2,128)(2,1)S(1)} %collective-permute-done.13), channel_id=1, source_target_pairs={{0,15},{1,0},{2,1},{3,2},{4,3},{5,4},{6,5},{7,6},{8,7},{9,8},{10,9... | collective-permute-start | bytes 12296 | tf_op jit(solution)/shard_map/ppermute | solution.py:23
  118.6 0.7 collective-permute-done.6
  119.5 0.8 dynamic_slice.17
  120.5 0.2 fusion.33
  120.7 4.4 %collective-permute-done.7 = bf16[1,2048]{1,0:T(2,128)(2,1)S(1)} collective-permute-done((bf16[1,2048]{1,0:T(2,128)(2,1)S(1)}, bf16[1,2048]{1,0:T(2,128)(2,1)S(1)}, u32[]{:S(2)}, u32[]{:S(2)}) %collective-permute-start.7) | collective-permute-done | bytes 4128 | tf_op jit(solution)/shard_map/ppermute | solution.py:21
  125.1 0.4 concatenate.20
  125.5 1.2 convolution_convert_fusion.2
  126.9 29.5 %all-reduce.2 = (f32[16]{0:T(128)S(1)}, f32[16]{0:T(128)S(1)}) all-reduce(f32[16]{0:T(128)S(1)} %get-tuple-element.6, f32[16]{0:T(128)S(1)} %get-tuple-element.5), channel_id=1, replica_groups=mesh['grp'=2,'ep'=16] {'ep'}, use_global_device_ids=true, to_apply=%region_7.8 | all-reduce | flops 32 | bytes 256 | tf_op jit(solution)/shard_map/psum | solution.py:135
  156.5 17.3 %all_gather.3 = bf16[16,2048]{1,0:T(8,128)(2,1)S(1)} all-gather(bf16[16,128]{1,0:T(8,128)(2,1)S(1)} %multiply_convert_fusion.1), channel_id=1, replica_groups=mesh['grp'=2,'ep'=16] {'ep'}, dimensions={1}, use_global_device_ids=true | all-gather | bytes 69632 | tf_op jit(solution)/shard_map/all_gather | solution.py:140
  173.9 0.2 fusion.9
  174.2 1.3 convolution_convert_fusion
  175.5 3.6 %all-to-all-start = ((bf16[8,16,128]{2,0,1:T(8,128)(2,1)}), bf16[8,16,128]{2,0,1:T(8,128)(2,1)S(1)}, u32[]{:S(2)}, u32[]{:S(2)}) async-start(bf16[8,16,128]{2,0,1:T(8,128)(2,1)} %bitcast.13), calls=%async_computation | async-start | bytes 65536 | tf_op jit(solution)/shard_map/all_to_all | solution.py:153
  179.2 0.2 fusion.52
  179.4 1.2 fusion.5
  180.6 5.1 %all-to-all-done = bf16[8,16,128]{2,0,1:T(8,128)(2,1)S(1)} async-done(((bf16[8,16,128]{2,0,1:T(8,128)(2,1)}), bf16[8,16,128]{2,0,1:T(8,128)(2,1)S(1)}, u32[]{:S(2)}, u32[]{:S(2)}) %all-to-all-start) | async-done | bytes 32800 | tf_op jit(solution)/shard_map/all_to_all | solution.py:153
  185.7 0.4 fusion.47
  186.1 29.7 %all-reduce.1 = (f32[16]{0:T(128)S(1)}, f32[16]{0:T(128)S(1)}) all-reduce(f32[16]{0:T(128)S(1)} %get-tuple-element.4, f32[16]{0:T(128)S(1)} %get-tuple-element.3), channel_id=1, replica_groups=mesh['grp'=2,'ep'=16] {'ep'}, use_global_device_ids=true, to_apply=%region_14.15 | all-reduce | flops 32 | bytes 256 | tf_op jit(solution)/shard_map/psum | solution.py:168
  215.8 0.7 copy-done.13
  216.4 0.7 multiply_convert_fusion
  (79 shorter events, 2.2 us)
Async XLA Ops:
  0.6 173.5 %copy-start = (bf16[1,256,2048]{2,1,0:T(8,128)(2,1)S(1)}, bf16[1,256,2048]{2,1,0:T(8,128)(2,1)}, u32[]{:S(2)}) copy-start(bf16[1,256,2048]{2,1,0:T(8,128)(2,1)} %param.43) | copy-start | bytes 3145732
  0.6 0.8 copy-start.7
  0.7 2.1 copy-start.6
  1.4 74.1 %copy-start.1 = (f32[1,32,64,128]{3,2,1,0:T(8,128)S(1)}, f32[1,32,64,128]{3,2,1,0:T(8,128)}, u32[]{:S(2)}) copy-start(f32[1,32,64,128]{3,2,1,0:T(8,128)} %param.26) | copy-start | bytes 3145732
  71.9 0.7 copy-start.17
  73.1 0.7 copy-start.9
  73.8 0.7 copy-start.8
  74.7 0.7 copy-start.14
  74.7 0.7 copy-start.15
  75.5 1.6 copy-start.16
  75.5 3.3 %copy-start.11 = (f32[2048]{0:T(1024)S(1)}, f32[2048]{0:T(1024)}, u32[]{:S(2)}) copy-start(f32[2048]{0:T(1024)} %param.36) | copy-start | bytes 24580
  75.5 32.3 %copy-start.10 = (s32[16,4]{0,1:T(4,128)S(1)}, s32[16,4]{0,1:T(4,128)}, u32[]{:S(2)}) copy-start(s32[16,4]{0,1:T(4,128)} %param.39) | copy-start | bytes 772
  75.5 43.8 %copy-start.12 = (f32[16,4]{0,1:T(4,128)S(1)}, f32[16,4]{0,1:T(4,128)}, u32[]{:S(2)}) copy-start(f32[16,4]{0,1:T(4,128)} %param.40) | copy-start | bytes 772
  76.9 97.0 %copy-start.2 = (bf16[1,2048,256]{2,1,0:T(8,128)(2,1)S(1)}, bf16[1,2048,256]{2,1,0:T(8,128)(2,1)}, u32[]{:S(2)}) copy-start(bf16[1,2048,256]{2,1,0:T(8,128)(2,1)} %param.41) | copy-start | bytes 3145732
  78.9 5.8 %collective-permute-start = (bf16[1,2048]{1,0:T(2,128)(2,1)S(1)}, bf16[1,2048]{1,0:T(2,128)(2,1)S(1)}, u32[]{:S(2)}, u32[]{:S(2)}) collective-permute-start(bf16[1,2048]{1,0:T(2,128)(2,1)S(1)} %convert_element_type.70), channel_id=1, source_target_pairs={{0,1},{1,2},{2,3},{3,4},{4,5},{5,6},{6,7},{7,8},{8,9},{9,10},{10,1... | collective-permute-start | bytes 12296 | tf_op jit(solution)/shard_map/ppermute | solution.py:21
  78.9 5.8 %collective-permute-start.8 = (bf16[1,2048]{1,0:T(2,128)(2,1)S(1)}, bf16[1,2048]{1,0:T(2,128)(2,1)S(1)}, u32[]{:S(2)}, u32[]{:S(2)}) collective-permute-start(bf16[1,2048]{1,0:T(2,128)(2,1)S(1)} %convert_element_type.70), channel_id=1, source_target_pairs={{0,15},{1,0},{2,1},{3,2},{4,3},{5,4},{6,5},{7,6},{8,7},{9,8},{10,9... | collective-permute-start | bytes 12296 | tf_op jit(solution)/shard_map/ppermute | solution.py:23
  84.7 5.8 %collective-permute-start.1 = (bf16[1,2048]{1,0:T(2,128)(2,1)S(1)}, bf16[1,2048]{1,0:T(2,128)(2,1)S(1)}, u32[]{:S(2)}, u32[]{:S(2)}) collective-permute-start(bf16[1,2048]{1,0:T(2,128)(2,1)S(1)} %collective-permute-done), channel_id=1, source_target_pairs={{0,1},{1,2},{2,3},{3,4},{4,5},{5,6},{6,7},{7,8},{8,9},{9,10},{10,1... | collective-permute-start | bytes 12296 | tf_op jit(solution)/shard_map/ppermute | solution.py:21
  84.7 5.8 %collective-permute-start.9 = (bf16[1,2048]{1,0:T(2,128)(2,1)S(1)}, bf16[1,2048]{1,0:T(2,128)(2,1)S(1)}, u32[]{:S(2)}, u32[]{:S(2)}) collective-permute-start(bf16[1,2048]{1,0:T(2,128)(2,1)S(1)} %collective-permute-done.8), channel_id=1, source_target_pairs={{0,15},{1,0},{2,1},{3,2},{4,3},{5,4},{6,5},{7,6},{8,7},{9,8},{10,9... | collective-permute-start | bytes 12296 | tf_op jit(solution)/shard_map/ppermute | solution.py:23
  90.5 5.8 %collective-permute-start.2 = (bf16[1,2048]{1,0:T(2,128)(2,1)S(1)}, bf16[1,2048]{1,0:T(2,128)(2,1)S(1)}, u32[]{:S(2)}, u32[]{:S(2)}) collective-permute-start(bf16[1,2048]{1,0:T(2,128)(2,1)S(1)} %collective-permute-done.1), channel_id=1, source_target_pairs={{0,1},{1,2},{2,3},{3,4},{4,5},{5,6},{6,7},{7,8},{8,9},{9,10},{10,1... | collective-permute-start | bytes 12296 | tf_op jit(solution)/shard_map/ppermute | solution.py:21
  90.5 5.8 %collective-permute-start.10 = (bf16[1,2048]{1,0:T(2,128)(2,1)S(1)}, bf16[1,2048]{1,0:T(2,128)(2,1)S(1)}, u32[]{:S(2)}, u32[]{:S(2)}) collective-permute-start(bf16[1,2048]{1,0:T(2,128)(2,1)S(1)} %collective-permute-done.9), channel_id=1, source_target_pairs={{0,15},{1,0},{2,1},{3,2},{4,3},{5,4},{6,5},{7,6},{8,7},{9,8},{10,9... | collective-permute-start | bytes 12296 | tf_op jit(solution)/shard_map/ppermute | solution.py:23
  96.2 5.8 %collective-permute-start.3 = (bf16[1,2048]{1,0:T(2,128)(2,1)S(1)}, bf16[1,2048]{1,0:T(2,128)(2,1)S(1)}, u32[]{:S(2)}, u32[]{:S(2)}) collective-permute-start(bf16[1,2048]{1,0:T(2,128)(2,1)S(1)} %collective-permute-done.2), channel_id=1, source_target_pairs={{0,1},{1,2},{2,3},{3,4},{4,5},{5,6},{6,7},{7,8},{8,9},{9,10},{10,1... | collective-permute-start | bytes 12296 | tf_op jit(solution)/shard_map/ppermute | solution.py:21
  96.3 6.4 %collective-permute-start.11 = (bf16[1,2048]{1,0:T(2,128)(2,1)S(1)}, bf16[1,2048]{1,0:T(2,128)(2,1)S(1)}, u32[]{:S(2)}, u32[]{:S(2)}) collective-permute-start(bf16[1,2048]{1,0:T(2,128)(2,1)S(1)} %collective-permute-done.10), channel_id=1, source_target_pairs={{0,15},{1,0},{2,1},{3,2},{4,3},{5,4},{6,5},{7,6},{8,7},{9,8},{10,9... | collective-permute-start | bytes 12296 | tf_op jit(solution)/shard_map/ppermute | solution.py:23
  102.0 5.8 %collective-permute-start.4 = (bf16[1,2048]{1,0:T(2,128)(2,1)S(1)}, bf16[1,2048]{1,0:T(2,128)(2,1)S(1)}, u32[]{:S(2)}, u32[]{:S(2)}) collective-permute-start(bf16[1,2048]{1,0:T(2,128)(2,1)S(1)} %collective-permute-done.3), channel_id=1, source_target_pairs={{0,1},{1,2},{2,3},{3,4},{4,5},{5,6},{6,7},{7,8},{8,9},{9,10},{10,1... | collective-permute-start | bytes 12296 | tf_op jit(solution)/shard_map/ppermute | solution.py:21
  102.7 5.8 %collective-permute-start.12 = (bf16[1,2048]{1,0:T(2,128)(2,1)S(1)}, bf16[1,2048]{1,0:T(2,128)(2,1)S(1)}, u32[]{:S(2)}, u32[]{:S(2)}) collective-permute-start(bf16[1,2048]{1,0:T(2,128)(2,1)S(1)} %collective-permute-done.11), channel_id=1, source_target_pairs={{0,15},{1,0},{2,1},{3,2},{4,3},{5,4},{6,5},{7,6},{8,7},{9,8},{10,9... | collective-permute-start | bytes 12296 | tf_op jit(solution)/shard_map/ppermute | solution.py:23
  107.8 5.8 %collective-permute-start.5 = (bf16[1,2048]{1,0:T(2,128)(2,1)S(1)}, bf16[1,2048]{1,0:T(2,128)(2,1)S(1)}, u32[]{:S(2)}, u32[]{:S(2)}) collective-permute-start(bf16[1,2048]{1,0:T(2,128)(2,1)S(1)} %collective-permute-done.4), channel_id=1, source_target_pairs={{0,1},{1,2},{2,3},{3,4},{4,5},{5,6},{6,7},{7,8},{8,9},{9,10},{10,1... | collective-permute-start | bytes 12296 | tf_op jit(solution)/shard_map/ppermute | solution.py:21
  108.5 5.8 %collective-permute-start.13 = (bf16[1,2048]{1,0:T(2,128)(2,1)S(1)}, bf16[1,2048]{1,0:T(2,128)(2,1)S(1)}, u32[]{:S(2)}, u32[]{:S(2)}) collective-permute-start(bf16[1,2048]{1,0:T(2,128)(2,1)S(1)} %collective-permute-done.12), channel_id=1, source_target_pairs={{0,15},{1,0},{2,1},{3,2},{4,3},{5,4},{6,5},{7,6},{8,7},{9,8},{10,9... | collective-permute-start | bytes 12296 | tf_op jit(solution)/shard_map/ppermute | solution.py:23
  113.6 5.8 %collective-permute-start.6 = (bf16[1,2048]{1,0:T(2,128)(2,1)S(1)}, bf16[1,2048]{1,0:T(2,128)(2,1)S(1)}, u32[]{:S(2)}, u32[]{:S(2)}) collective-permute-start(bf16[1,2048]{1,0:T(2,128)(2,1)S(1)} %collective-permute-done.5), channel_id=1, source_target_pairs={{0,1},{1,2},{2,3},{3,4},{4,5},{5,6},{6,7},{7,8},{8,9},{9,10},{10,1... | collective-permute-start | bytes 12296 | tf_op jit(solution)/shard_map/ppermute | solution.py:21
  114.2 6.4 %collective-permute-start.14 = (bf16[1,2048]{1,0:T(2,128)(2,1)S(1)}, bf16[1,2048]{1,0:T(2,128)(2,1)S(1)}, u32[]{:S(2)}, u32[]{:S(2)}) collective-permute-start(bf16[1,2048]{1,0:T(2,128)(2,1)S(1)} %collective-permute-done.13), channel_id=1, source_target_pairs={{0,15},{1,0},{2,1},{3,2},{4,3},{5,4},{6,5},{7,6},{8,7},{9,8},{10,9... | collective-permute-start | bytes 12296 | tf_op jit(solution)/shard_map/ppermute | solution.py:23
  119.3 5.8 %collective-permute-start.7 = (bf16[1,2048]{1,0:T(2,128)(2,1)S(1)}, bf16[1,2048]{1,0:T(2,128)(2,1)S(1)}, u32[]{:S(2)}, u32[]{:S(2)}) collective-permute-start(bf16[1,2048]{1,0:T(2,128)(2,1)S(1)} %collective-permute-done.6), channel_id=1, source_target_pairs={{0,1},{1,2},{2,3},{3,4},{4,5},{5,6},{6,7},{7,8},{8,9},{9,10},{10,1... | collective-permute-start | bytes 12296 | tf_op jit(solution)/shard_map/ppermute | solution.py:21
  120.6 53.5 %copy-start.3 = (bf16[1,2048,256]{2,1,0:T(8,128)(2,1)S(1)}, bf16[1,2048,256]{2,1,0:T(8,128)(2,1)}, u32[]{:S(2)}) copy-start(bf16[1,2048,256]{2,1,0:T(8,128)(2,1)} %param.42) | copy-start | bytes 3145732
  174.2 5.0 %copy-start.4 = (bf16[2048,256]{1,0:T(8,128)(2,1)S(1)}, bf16[2048,256]{1,0:T(8,128)(2,1)}, u32[]{:S(2)}) copy-start(bf16[2048,256]{1,0:T(8,128)(2,1)} %param.44) | copy-start | bytes 3145732
  175.5 3.9 %copy-start.5 = (bf16[2048,256]{1,0:T(8,128)(2,1)S(1)}, bf16[2048,256]{1,0:T(8,128)(2,1)}, u32[]{:S(2)}) copy-start(bf16[2048,256]{1,0:T(8,128)(2,1)} %param.45) | copy-start | bytes 3145732
  175.5 10.2 %all-to-all-start = ((bf16[8,16,128]{2,0,1:T(8,128)(2,1)}), bf16[8,16,128]{2,0,1:T(8,128)(2,1)S(1)}, u32[]{:S(2)}, u32[]{:S(2)}) async-start(bf16[8,16,128]{2,0,1:T(8,128)(2,1)} %bitcast.13), calls=%async_computation | async-start | bytes 65536 | tf_op jit(solution)/shard_map/all_to_all | solution.py:153
  215.8 0.7 copy-start.13
